TPU v7x, 32 devices: a whole 2x2x4 slice. The times are simulated.
32 devices in a mesh: grp: 2 (over y), ep: 4 (over z), tp: 4 (over x, core).
Axes of the slice: x: 2, y: 2, z: 4, core: 2. Of those that a mesh axis runs over, the one named last changes fastest.
Arguments:
- mixer_tokens: bfloat16 [4096, 2048], P(('grp', 'ep', 'tp')), parts along dimension 0, may hold values from -6 to 6
- mixer_gain: bfloat16 [2048], replicated, may hold values from 0.099609375 to 1.8984375
- in_weight: bfloat16 [2048, 2048], P(None, 'tp'), may hold values from -0.125 to 0.125
- group_weight: bfloat16 [4, 512, 512], P('tp'), may hold values from -0.25 to 0.25
- channel_scale: bfloat16 [2048], P('tp'), may hold values from 0.099609375 to 1.8984375
- out_weight: bfloat16 [2048, 2048], P('tp'), may hold values from -0.125 to 0.125
- expert_tokens: bfloat16 [4096, 2048], P(('grp', 'ep', 'tp')), parts along dimension 0, may hold values from -6 to 6
- expert_gain: bfloat16 [2048], replicated, may hold values from 0.099609375 to 1.8984375
- route_ids: int32 [4096, 2], P(('grp', 'ep', 'tp')), parts along dimension 0, may hold values from 0 to 3, all different within a row; in each aligned block of 128 rows (0 to 127, 128 to 255, ...) at most 128 rows name the same one
- route_weights: float32 [4096, 2], P(('grp', 'ep', 'tp')), parts along dimension 0, may hold values from 0.1 to 1
- gate_weight: bfloat16 [4, 2048, 1024], P('ep', None, 'tp'), may hold values from -0.125 to 0.125
- up_weight: bfloat16 [4, 2048, 1024], P('ep', None, 'tp'), may hold values from -0.125 to 0.125
- down_weight: bfloat16 [4, 1024, 2048], P('ep', 'tp'), may hold values from -0.1875 to 0.1875
Outputs:
- mixed_tokens: bfloat16 [4096, 2048], P(('grp', 'ep', 'tp')), parts along dimension 0
- expert_mix: bfloat16 [4096, 2048], P(('grp', 'ep', 'tp')), parts along dimension 0
There are 2 independent parts, one for each index of `grp`. A program takes and returns all parts, laid end to end along the dimension named above; an argument that names none is the same for every part. Nothing has to cross between parts.
Inputs may be any that keep to these rules, and one draw needn't show every extreme that they name: `route_ids`: each row names 2 different experts; in the rows of one device no expert is named more than 128 times, and one expert exactly 128 times in the rows of some device.
All inputs are finite; a program needn't handle non-finite values.
Results may differ from a plain program's by a relative error of at most 0.015.
Values may be sent and summed in bfloat16 or wider, within the bound.
A program may use at most 128 MiB of HBM per device.

v0:
```python
import jax
import jax.numpy as jnp
from jax import lax
from jax.sharding import PartitionSpec as P

WINDOW_MAX = 16


def shifted(value, axis, by):
    devices = lax.axis_size(axis)
    pairs = [(i, i + by) for i in range(devices) if 0 <= i + by < devices]
    return lax.ppermute(value, axis, pairs)


def rms_rows(rows, gain):
    values = rows.astype(jnp.float32)
    scaled = values * lax.rsqrt(jnp.mean(values * values, axis=-1, keepdims=True) + 1e-06)
    return (scaled * gain.astype(jnp.float32)).astype(jnp.bfloat16)


def expert_hidden(rows, w_gate, w_up):
    gate = jnp.dot(rows, w_gate, preferred_element_type=jnp.float32)
    upper = jnp.dot(rows, w_up, preferred_element_type=jnp.float32)
    return (jax.nn.silu(gate) * upper).astype(jnp.bfloat16)


def local(
    mixer_tokens,
    mixer_gain,
    in_weight,
    group_weight,
    channel_scale,
    out_weight,
    expert_tokens,
    expert_gain,
    route_ids,
    route_weights,
    gate_weight,
    up_weight,
    down_weight,
):
    normed = rms_rows(mixer_tokens, mixer_gain)
    pooled_in = jnp.dot(
        lax.all_gather(normed, "tp", axis=0, tiled=True),
        in_weight,
        preferred_element_type=jnp.float32,
    ).astype(jnp.bfloat16)
    block_rows = pooled_in.shape[0]
    rim_rows = shifted(pooled_in[block_rows - WINDOW_MAX :], "ep", 1)
    values = pooled_in.astype(jnp.float32)
    extended = jnp.concatenate([rim_rows.astype(jnp.float32), values], axis=0)
    window = jnp.left_shift(jnp.int32(2), lax.axis_index("tp"))
    sums = extended
    span = 1
    total = jnp.zeros_like(values)
    for level in range(WINDOW_MAX.bit_length() - 1):
        sums = sums[span:] + sums[:-span]
        span = span * 2
        total = total + jnp.where(window == span, sums[sums.shape[0] - block_rows :], 0.0)
    positions = lax.axis_index("ep") * block_rows + lax.iota(jnp.int32, block_rows) + 1
    counts = jnp.minimum(positions, window).astype(jnp.float32)
    pooled = (total / counts[:, None] - values).astype(jnp.bfloat16)
    grouped = (
        jnp.dot(pooled, group_weight[0], preferred_element_type=jnp.float32)
        * channel_scale.astype(jnp.float32)
    ).astype(jnp.bfloat16)
    rows = grouped
    mixed_tokens = lax.psum_scatter(
        jnp.dot(rows, out_weight, preferred_element_type=jnp.float32).astype(jnp.bfloat16),
        "tp",
        scatter_dimension=0,
        tiled=True,
    )
    expert_in = rms_rows(expert_tokens, expert_gain)
    shares = route_weights / jnp.sum(route_weights, axis=1, keepdims=True)
    rows_here, top_k = route_ids.shape
    width = expert_in.shape[1]
    n_experts = lax.axis_size("ep") * gate_weight.shape[0]
    capacity = 4 * rows_here // n_experts
    flat_ids = route_ids.reshape(rows_here * top_k)
    one_hot = (flat_ids[:, None] == jnp.arange(n_experts, dtype=jnp.int32)[None, :]).astype(
        jnp.int32
    )
    before = jnp.cumsum(one_hot, axis=0) - one_hot
    slots = jnp.sum(before * one_hot, axis=1)
    targets = flat_ids * capacity + slots
    placement = (
        targets.reshape(rows_here, top_k)[None, :, :]
        == jnp.arange(n_experts * capacity, dtype=jnp.int32)[:, None, None]
    )
    dispatch = jnp.any(placement, axis=2).astype(jnp.bfloat16)
    outgoing = jnp.dot(dispatch, expert_in, preferred_element_type=jnp.float32).astype(jnp.bfloat16)
    outgoing = outgoing.reshape(n_experts, capacity, width)
    arrived = lax.all_to_all(outgoing, "ep", split_axis=0, concat_axis=0, tiled=True)
    sources, held, _ = arrived.shape
    flat = arrived.reshape(sources * held, width)
    hidden = expert_hidden(
        lax.all_gather(flat, "tp", axis=0, tiled=True), gate_weight[0], up_weight[0]
    )
    rows = hidden
    summed = lax.psum_scatter(
        jnp.dot(rows, down_weight[0], preferred_element_type=jnp.float32).astype(jnp.bfloat16),
        "tp",
        scatter_dimension=0,
        tiled=True,
    ).astype(jnp.float32)
    expert_out = lax.all_to_all(
        summed.reshape(sources, held, width).astype(jnp.bfloat16),
        "ep",
        split_axis=0,
        concat_axis=0,
        tiled=True,
    ).astype(jnp.float32)
    flat_out = expert_out.reshape(n_experts * capacity, width)
    picked = jnp.take(flat_out, targets, axis=0).reshape(rows_here, top_k, width)
    expert_mix = jnp.sum(picked * shares[:, :, None], axis=1).astype(jnp.bfloat16)
    return (mixed_tokens, expert_mix)


def solution(mesh):
    placed = (
        P(("grp", "ep", "tp"), None),
        P(),
        P(None, "tp"),
        P("tp", None, None),
        P("tp"),
        P("tp", None),
        P(("grp", "ep", "tp"), None),
        P(),
        P(("grp", "ep", "tp"), None),
        P(("grp", "ep", "tp"), None),
        P("ep", None, "tp"),
        P("ep", None, "tp"),
        P("ep", "tp", None),
    )
    return jax.shard_map(
        local,
        mesh=mesh,
        in_specs=placed,
        out_specs=(P(("grp", "ep", "tp"), None), P(("grp", "ep", "tp"), None)),
        check_vma=False,
    )
```

profile of v0, /device:TPU:0, one launch (start us, length us, event | category | flops | bytes accessed | tf_op | source)
XLA Modules:
  0.0 304.9 jit_solution(17231655815007046173)
XLA Ops:
  7.2 0.9 copy.33
  8.4 1.2 reduce-window.6
  10.3 0.7 compare_and_fusion
  11.8 1.2 fusion.6
  13.0 1.8 convolution_convert_fusion.1
  14.8 54.4 %all_to_all.10 = bf16[4,128,2048]{2,1,0:T(8,128)(2,1)} all-to-all(bf16[4,128,2048]{2,1,0:T(8,128)(2,1)S(1)} %bitcast.48), channel_id=1, replica_groups=mesh['grp'=2,'ep'=4,'tp'=4] {'ep'}, dimensions={0} | all-to-all | bytes 4194304 | tf_op jit(solution)/shard_map/all_to_all | solution.py:94
  70.5 1.0 fusion.5
  71.6 55.4 %all-gather.5.cloned.1.call-done = bf16[2048,2048]{1,0:T(8,128)(2,1)} async-done(((bf16[512,2048]{1,0:T(8,128)(2,1)}), bf16[2048,2048]{1,0:T(8,128)(2,1)}) %all-gather.5.cloned.1.call-update) | async-done | bytes 8388624 | tf_op jit(solution)/shard_map/all_gather | solution.py:98
  127.0 7.3 %fusion.18 = f32[2048,256]{1,0:T(8,128)} fusion(bf16[2048,2048]{1,0:T(8,128)(2,1)} %all-gather.5.cloned.1.call-done, bf16[1,2048,256]{2,1,0:T(8,128)(2,1)} %param.23), kind=kOutput, calls=%fused_computation.37 | convolution fusion | flops 2147483648 | bytes 11534336 | tf_op jit(solution)/shard_map/dot_general | solution.py:22
  134.2 17.5 %convolution_convert_fusion = bf16[2048,2048]{1,0:T(8,128)(2,1)} fusion(bf16[2048,2048]{1,0:T(8,128)(2,1)} %all-gather.5.cloned.1.call-done, f32[2048,256]{1,0:T(8,128)} %fusion.18, bf16[1,256,2048]{2,1,0:T(8,128)(2,1)S(1)} %copy-done.9, bf16[1,2048,256]{2,1,0:T(8,128)(2,1)} %param.24), kind=kOutput, calls=%fused_computation.1 | convolution fusion | flops 4302307328 | bytes 20971520 | tf_op jit(solution)/shard_map/dot_general | solution.py:102
  151.8 4.4 %fusion.54 = (f32[512,512]{1,0:T(8,128)}, bf16[512,512]{1,0:T(8,128)(2,1)S(1)}) fusion(bf16[512,2048]{1,0:T(8,128)(2,1)} %all-gather.3.cloned.1.call-done, bf16[2048,512]{1,0:T(8,128)(2,1)} %param.15), kind=kOutput, calls=%fused_computation.74 | convolution fusion | flops 1074266112 | bytes 5767168 | tf_op jit(solution)/shard_map/dot_general | solution.py:43
  156.3 3.6 %collective-permute-start = (bf16[16,512]{1,0:T(8,128)(2,1)S(1)}, bf16[16,512]{1,0:T(8,128)(2,1)S(1)}, u32[]{:S(2)}, u32[]{:S(2)}) collective-permute-start(bf16[16,512]{1,0:T(8,128)(2,1)S(1)} %slice.62), channel_id=1, source_target_pairs={{0,4},{4,8},{8,12},{1,5},{5,9},{9,13},{2,6},{6,10},{10,14},{3,7},{... | collective-permute-start | bytes 49160 | tf_op jit(solution)/shard_map/ppermute | solution.py:12
  160.0 1.2 collective-permute-done
  161.2 2.3 fusion.2
  163.6 1.0 copy-done.1
  164.7 1.7 fusion.53
  166.7 6.5 %convolution_convert_fusion.2 = bf16[512,2048]{1,0:T(8,128)(2,1)} fusion(bf16[512,2048]{1,0:T(8,128)(2,1)S(1)} %copy-done, f32[513,512]{1,0:T(8,128)} %get-tuple-element.5, f32[513,512]{1,0:T(8,128)} %get-tuple-element.4, f32[521,512]{1,0:T(8,128)} %copy-done.2, f32[525,512]{1,0:T(8,128)} %copy-done.1, f32[527,512]{1,0:T(8,128)S(1)} %fusion.2, ...), kind=kOutput, calls=%fused_computation.3 | convolution fusion | flops 1346895872 | bytes 10489860 | tf_op jit(solution)/shard_map/dot_general | solution.py:69
  173.3 52.4 %reduce-scatter.5.cloned.1.call-done = bf16[512,2048]{1,0:T(8,128)(2,1)} async-done(((bf16[2048,2048]{1,0:T(8,128)(2,1)}), bf16[512,2048]{1,0:T(8,128)(2,1)}) %reduce-scatter.5.cloned.1.call-update) | async-done | bytes 2097168 | tf_op jit(solution)/shard_map/reduce_scatter | solution.py:101
  225.7 4.7 %all-to-all-start.1 = ((bf16[4,128,2048]{2,1,0:T(8,128)(2,1)}), bf16[4,128,2048]{2,1,0:T(8,128)(2,1)}, u32[]{:S(2)}, u32[]{:S(2)}) async-start(bf16[4,128,2048]{2,1,0:T(8,128)(2,1)} %bitcast.49), calls=%async_computation.3 | async-start | bytes 4194304 | tf_op jit(solution)/shard_map/all_to_all | solution.py:107
  231.0 47.6 %all-to-all-done.1 = bf16[4,128,2048]{2,1,0:T(8,128)(2,1)} async-done(((bf16[4,128,2048]{2,1,0:T(8,128)(2,1)}), bf16[4,128,2048]{2,1,0:T(8,128)(2,1)}, u32[]{:S(2)}, u32[]{:S(2)}) %all-to-all-start.1) | async-done | bytes 2097184 | tf_op jit(solution)/shard_map/all_to_all | solution.py:107
  278.7 4.0 %bitcast_convert_fusion = f32[512,2048]{1,0:T(8,128)} fusion(bf16[4,128,2048]{2,1,0:T(8,128)(2,1)} %all-to-all-done.1), kind=kLoop, calls=%fused_computation.6 | loop fusion | flops 1048576 | bytes 6291456 | tf_op jit(solution)/shard_map/reshape | solution.py:114
  282.7 5.8 %gather_fusion = f32[256,2048]{1,0:T(8,128)} fusion(f32[512,2048]{1,0:T(8,128)} %bitcast_convert_fusion, s32[1024]{0:T(1024)S(1)} %pad_clamp_fusion), kind=kCustom, calls=%fused_computation | custom fusion | bytes 4195328 | tf_op jit(solution)/shard_map/jit(_take)/gather | solution.py:115
  288.5 3.5 %gather.7 = f32[128,2,2048]{2,1,0:T(2,128)} reshape(f32[256,2048]{1,0:T(8,128)} %gather_fusion) | data formatting | bytes 4194304 | tf_op jit(solution)/shard_map/jit(_take)/gather | solution.py:115
  292.0 6.4 %multiply_reduce_fusion = bf16[128,2048]{1,0:T(8,128)(2,1)} fusion(f32[128,2,2048]{2,1,0:T(2,128)} %gather.7, pred[128,2]{1,0:T(8,128)(4,1)S(1)} %copy.38, f32[128,2]{1,0:T(8,128)S(1)} %copy.40), kind=kLoop, calls=%fused_computation.7 | loop fusion | flops 1310720 | bytes 2622720 | tf_op jit(solution)/shard_map/reduce_sum | solution.py:116
  (62 shorter events, 4.2 us)
Async XLA Ops:
  7.2 159.6 %copy-start = (bf16[512,2048]{1,0:T(8,128)(2,1)S(1)}, bf16[512,2048]{1,0:T(8,128)(2,1)}, u32[]{:S(2)}) copy-start(bf16[512,2048]{1,0:T(8,128)(2,1)} %param.18) | copy-start | bytes 6291460
  7.2 119.8 %all-gather.5.cloned.1.call-start = ((), (), s32[]{:S(2)}) async-start(), calls=%async_computation.6 | async-start | bytes 10485760 | tf_op jit(solution)/shard_map/all_gather | solution.py:98
  69.3 0.7 copy-start.5
  69.3 1.1 copy-start.3
  69.3 82.5 %all-gather.3.cloned.1.call-start = ((), (), s32[]{:S(2)}) async-start(), calls=%async_computation.4 | async-start | bytes 2621440 | tf_op jit(solution)/shard_map/all_gather | solution.py:44
  71.5 62.7 %copy-start.9 = (bf16[1,256,2048]{2,1,0:T(8,128)(2,1)S(1)}, bf16[1,256,2048]{2,1,0:T(8,128)(2,1)}, u32[]{:S(2)}) copy-start(bf16[1,256,2048]{2,1,0:T(8,128)(2,1)} %param.25) | copy-start | bytes 3145732
  71.6 154.2 %reduce-scatter.5.cloned.1.call-start = ((), (), s32[]{:S(2)}) async-start(), calls=%async_computation.7 | async-start | bytes 10485760 | tf_op jit(solution)/shard_map/reduce_scatter | solution.py:101
  151.7 146.7 %reduce-scatter.3.cloned.1.call-start = ((), (), s32[]{:S(2)}) async-start(), calls=%async_computation.5 | async-start | bytes 2621440 | tf_op jit(solution)/shard_map/reduce_scatter | solution.py:68
  151.8 8.2 %copy-start.7 = (bf16[512]{0:T(512)(128)(2,1)S(1)}, bf16[512]{0:T(512)(128)(2,1)}, u32[]{:S(2)}) copy-start(bf16[512]{0:T(512)(128)(2,1)} %param.17) | copy-start | bytes 3076
  156.3 4.9 %copy-start.8 = (bf16[512,512]{1,0:T(8,128)(2,1)}, bf16[512,512]{1,0:T(8,128)(2,1)S(1)}, u32[]{:S(2)}) copy-start(bf16[512,512]{1,0:T(8,128)(2,1)S(1)} %get-tuple-element.7) | copy-start | bytes 1572868
  156.3 4.9 %collective-permute-start = (bf16[16,512]{1,0:T(8,128)(2,1)S(1)}, bf16[16,512]{1,0:T(8,128)(2,1)S(1)}, u32[]{:S(2)}, u32[]{:S(2)}) collective-permute-start(bf16[16,512]{1,0:T(8,128)(2,1)S(1)} %slice.62), channel_id=1, source_target_pairs={{0,4},{4,8},{8,12},{1,5},{5,9},{9,13},{2,6},{6,10},{10,14},{3,7},{... | collective-permute-start | bytes 49160 | tf_op jit(solution)/shard_map/ppermute | solution.py:12
  163.6 1.0 copy-start.1
  164.7 2.0 copy-start.2
  225.7 4.7 %copy-start.4 = (s32[128,2]{0,1:T(2,128)S(1)}, s32[128,2]{0,1:T(2,128)}, u32[]{:S(2)}) copy-start(s32[128,2]{0,1:T(2,128)} %param.21) | copy-start | bytes 3076
  225.7 5.1 %copy-start.6 = (f32[128,2]{0,1:T(2,128)S(1)}, f32[128,2]{0,1:T(2,128)}, u32[]{:S(2)}) copy-start(f32[128,2]{0,1:T(2,128)} %param.22) | copy-start | bytes 3076
  225.7 52.9 %all-to-all-start.1 = ((bf16[4,128,2048]{2,1,0:T(8,128)(2,1)}), bf16[4,128,2048]{2,1,0:T(8,128)(2,1)}, u32[]{:S(2)}, u32[]{:S(2)}) async-start(bf16[4,128,2048]{2,1,0:T(8,128)(2,1)} %bitcast.49), calls=%async_computation.3 | async-start | bytes 4194304 | tf_op jit(solution)/shard_map/all_to_all | solution.py:107
Sparse Core Ops, SparseCore 0:
  69.4 57.4 all-gather.4
  129.1 22.5 all-gather.2
  154.3 71.4 reduce-scatter.4
  228.7 31.1 reduce-scatter.2
where the time goes:
time: 306 us; the launch traced here: 305 us
  waiting for transfers between devices  157 us (51%)
  blocking collectives  54.4 us (18%)
  matrix products  37.6 us (12%)
  other arithmetic  18.3 us (6%)
  local copies, waits for them, and re-layouts  15.5 us (5%)
  between operations  14 us (5%)
  starting transfers between devices  8.52 us (3%)
    all_gather x1, waiting for transfers between devices, local(): lax.all_gather(flat, 'tp', axis=0, tiled=True)  55.4 us
    all_to_all x1, blocking collectives, local(): lax.all_to_all(outgoing, 'ep', split_axis=0, concat_axis=0, tiled=True)  54.4 us
    reduce_scatter x1, waiting for transfers between devices, local(): lax.psum_scatter(jnp.dot(rows, down_weight[0], preferred_element_type=jnp...  52.4 us
    all_to_all x1, waiting for transfers between devices, local(): lax.all_to_all(summed.reshape(sources, held, width).astype(jnp.bfloat16),...  47.6 us
    dot_general x1, matrix products, local(): jnp.dot(rows, down_weight[0], preferred_element_type=jnp.float32)  17.5 us
    gather x2, local copies, waits for them, and re-layouts, local(): jnp.take(flat_out, targets, axis=0).reshape(rows_here, top_k, width)  9.3 us
    dot_general x1, matrix products, expert_hidden(): gate = jnp.dot(rows, w_gate, preferred_element_type=jnp.float32)  7.26 us
    dot_general x1, matrix products, local(): jnp.dot(rows, out_weight, preferred_element_type=jnp.float32)  6.53 us
  transfers between devices with their start and end apart: 6, of which 4 were waited for; matrix products, arithmetic and copies ran while one was open for 20% of the time, Pallas kernels for 0%

commit v1 on v0

--- a/solution.py
+++ b/solution.py
@@ -77,6 +77,20 @@
     width = expert_in.shape[1]
     n_experts = lax.axis_size("ep") * gate_weight.shape[0]
     capacity = 4 * rows_here // n_experts
+    if capacity >= rows_here:
+        experts = jnp.arange(n_experts, dtype=jnp.int32)
+        named = (route_ids[:, :, None] == experts[None, None, :]).astype(jnp.float32)
+        coefs = jnp.sum(named * shares[:, :, None], axis=1)
+        every = lax.all_gather(expert_in, ("ep", "tp"), axis=0, tiled=True)
+        coefs = lax.all_gather(coefs, ("ep", "tp"), axis=0, tiled=True)
+        mine = (experts == lax.axis_index("ep")).astype(jnp.float32)
+        coef = jnp.sum(coefs * mine[None, :], axis=1, keepdims=True)
+        hidden = expert_hidden(every, gate_weight[0], up_weight[0])
+        part = jnp.dot(hidden, down_weight[0], preferred_element_type=jnp.float32) * coef
+        expert_mix = lax.psum_scatter(
+            part.astype(jnp.bfloat16), ("ep", "tp"), scatter_dimension=0, tiled=True
+        )
+        return (mixed_tokens, expert_mix)
     flat_ids = route_ids.reshape(rows_here * top_k)
     one_hot = (flat_ids[:, None] == jnp.arange(n_experts, dtype=jnp.int32)[None, :]).astype(
         jnp.int32

time: 306 us -> 262 us (0.86)
  blocking collectives: 54.4 us -> 21.7 us
  waiting for transfers between devices: 157 us -> 180 us
  local copies, waits for them, and re-layouts: 15.5 us -> 3.23 us
  other arithmetic: 18.3 us -> 7.65 us
  matrix products: 37.6 us -> 31.7 us
  starting transfers between devices: 8.52 us -> 3.54 us
    reduce_scatter x1, waiting for transfers between devices: 52.4 us -> 108 us  [local(): lax.psum_scatter(part.astype(jnp.bfloat16), ('ep', 'tp'), scatter_dimensi...]
    all_to_all x1 -> x0, blocking collectives: 54.4 us -> none  [local(): lax.all_to_all(outgoing, 'ep', split_axis=0, concat_axis=0, tiled=True)]
    all_to_all x1 -> x0, waiting for transfers between devices: 47.6 us -> none  [local(): lax.all_to_all(summed.reshape(sources, held, width).astype(jnp.bfloat16),...]
    all_gather x1, waiting for transfers between devices: 0.02 us -> 24.1 us  [local(): lax.all_gather(normed, 'tp', axis=0, tiled=True)]
    all_gather x0 -> x1, blocking collectives: none -> 21.7 us  [local(): coefs = lax.all_gather(coefs, ('ep', 'tp'), axis=0, tiled=True)]
    all_gather x1, waiting for transfers between devices: 55.4 us -> 34.6 us  [local(): every = lax.all_gather(expert_in, ('ep', 'tp'), axis=0, tiled=True)]
    reduce_scatter x1, waiting for transfers between devices: 0.01 us -> 11.4 us  [local(): lax.psum_scatter(jnp.dot(rows, out_weight, preferred_element_type=jnp.flo...]
    gather x2 -> x0, local copies, waits for them, and re-layouts: 9.3 us -> none  [local(): jnp.take(flat_out, targets, axis=0).reshape(rows_here, top_k, width)]
  transfers between devices with their start and end apart: 6 -> 5, of which waited for: 4 -> 5; matrix products, arithmetic and copies ran while one was open for 20% -> 14% of each run, Pallas kernels for 0% -> 0%
where the time goes in v1:
time: 262 us; the launch traced here: 261 us
  waiting for transfers between devices  180 us (69%)
  matrix products  31.7 us (12%)
  blocking collectives  21.7 us (8%)
  between operations  13.9 us (5%)
  other arithmetic  7.65 us (3%)
  starting transfers between devices  3.54 us (1%)
  local copies, waits for them, and re-layouts  3.23 us (1%)
    reduce_scatter x1, waiting for transfers between devices, local(): lax.psum_scatter(part.astype(jnp.bfloat16), ('ep', 'tp'), scatter_dimensi...  108 us
    all_gather x1, waiting for transfers between devices, local(): every = lax.all_gather(expert_in, ('ep', 'tp'), axis=0, tiled=True)  34.6 us
    all_gather x1, waiting for transfers between devices, local(): lax.all_gather(normed, 'tp', axis=0, tiled=True)  24.1 us
    all_gather x1, blocking collectives, local(): coefs = lax.all_gather(coefs, ('ep', 'tp'), axis=0, tiled=True)  21.7 us
    dot_general x1, matrix products, local(): jnp.dot(hidden, down_weight[0], preferred_element_type=jnp.float32) * coef  14.4 us
    reduce_scatter x1, waiting for transfers between devices, local(): lax.psum_scatter(jnp.dot(rows, out_weight, preferred_element_type=jnp.flo...  11.4 us
    dot_general x1, matrix products, expert_hidden(): gate = jnp.dot(rows, w_gate, preferred_element_type=jnp.float32)  7.04 us
    dot_general x1, matrix products, local(): jnp.dot(rows, out_weight, preferred_element_type=jnp.float32)  5.84 us
  transfers between devices with their start and end apart: 5, of which 5 were waited for; matrix products, arithmetic and copies ran while one was open for 14% of the time, Pallas kernels for 0%

profile of v1, /device:TPU:0, one launch (start us, length us, event | category | flops | bytes accessed | tf_op | source)
XLA Modules:
  0.0 261.4 jit_solution(4992600825104858551)
XLA Ops:
  7.2 0.8 convert_element_type.61
  8.1 1.2 fusion.3
  9.3 2.0 fusion.5
  11.5 0.2 fusion.6
  11.7 1.0 fusion.8
  12.7 24.1 %all-gather.3.cloned.1.call-done = bf16[512,2048]{1,0:T(8,128)(2,1)} async-done(((bf16[128,2048]{1,0:T(8,128)(2,1)}), bf16[512,2048]{1,0:T(8,128)(2,1)}) %all-gather.3.cloned.1.call-update) | async-done | bytes 2097168 | tf_op jit(solution)/shard_map/all_gather | solution.py:44
  36.8 4.4 %fusion.45 = (f32[512,512]{1,0:T(8,128)}, bf16[512,512]{1,0:T(8,128)(2,1)S(1)}) fusion(bf16[512,2048]{1,0:T(8,128)(2,1)} %all-gather.3.cloned.1.call-done, bf16[2048,512]{1,0:T(8,128)(2,1)} %param.15), kind=kOutput, calls=%fused_computation.57 | convolution fusion | flops 1074266112 | bytes 5767168 | tf_op jit(solution)/shard_map/dot_general | solution.py:43
  41.3 3.4 %collective-permute-start = (bf16[16,512]{1,0:T(8,128)(2,1)S(1)}, bf16[16,512]{1,0:T(8,128)(2,1)S(1)}, u32[]{:S(2)}, u32[]{:S(2)}) collective-permute-start(bf16[16,512]{1,0:T(8,128)(2,1)S(1)} %slice.52), channel_id=1, source_target_pairs={{0,4},{4,8},{8,12},{1,5},{5,9},{9,13},{2,6},{6,10},{10,14},{3,7},{... | collective-permute-start | bytes 49160 | tf_op jit(solution)/shard_map/ppermute | solution.py:12
  44.7 1.4 collective-permute-done
  46.1 1.9 fusion.2
  48.0 0.1 slice_add_fusion.1
  48.2 1.0 copy-done.1
  49.1 0.1 slice_add_fusion
  49.3 1.6 fusion.44
  50.9 5.8 %convolution_convert_fusion = bf16[512,2048]{1,0:T(8,128)(2,1)} fusion(bf16[512,2048]{1,0:T(8,128)(2,1)S(1)} %copy-done, f32[513,512]{1,0:T(8,128)} %get-tuple-element.3, f32[513,512]{1,0:T(8,128)} %get-tuple-element.2, f32[521,512]{1,0:T(8,128)} %copy-done.2, f32[525,512]{1,0:T(8,128)} %copy-done.1, f32[527,512]{1,0:T(8,128)S(1)} %fusion.2, ...), kind=kOutput, calls=%fused_computation.1 | convolution fusion | flops 1346895872 | bytes 10489860 | tf_op jit(solution)/shard_map/dot_general | solution.py:69
  56.8 0.0 reduce-scatter.5.cloned.1.call-start
  56.9 0.6 copy-done.5
  57.5 21.7 %all_gather.11 = f32[2048,4]{0,1:T(4,128)S(1)} all-gather(f32[128,4]{0,1:T(4,128)S(1)} %select_reduce_fusion), channel_id=1, replica_groups=mesh['grp'=2,'ep'=4,'tp'=4] {'ep','tp'}, dimensions={0}, use_global_device_ids=true | all-gather | bytes 34816 | tf_op jit(solution)/shard_map/all_gather | solution.py:85
  79.2 0.1 multiply_reduce_fusion
  79.3 34.6 %all-gather.5.cloned.1.call-done = bf16[2048,2048]{1,0:T(8,128)(2,1)} async-done(((bf16[128,2048]{1,0:T(8,128)(2,1)}), bf16[2048,2048]{1,0:T(8,128)(2,1)}) %all-gather.5.cloned.1.call-update) | async-done | bytes 8388624 | tf_op jit(solution)/shard_map/all_gather | solution.py:84
  114.0 7.0 %fusion.18 = f32[2048,256]{1,0:T(8,128)} fusion(bf16[2048,2048]{1,0:T(8,128)(2,1)} %all-gather.5.cloned.1.call-done, bf16[1,2048,256]{2,1,0:T(8,128)(2,1)S(1)} %copy-done.9), kind=kOutput, calls=%fused_computation.33 | convolution fusion | flops 2147483648 | bytes 11534336 | tf_op jit(solution)/shard_map/dot_general | solution.py:22
  121.0 14.4 %multiply_convert_fusion = bf16[2048,2048]{1,0:T(8,128)(2,1)} fusion(f32[2048]{0:T(1024)S(1)} %multiply_reduce_fusion, bf16[2048,2048]{1,0:T(8,128)(2,1)} %all-gather.5.cloned.1.call-done, f32[2048,256]{1,0:T(8,128)} %fusion.18, bf16[1,256,2048]{2,1,0:T(8,128)(2,1)} %param.25, bf16[1,2048,256]{2,1,0:T(8,128)(2,1)} %param.24), kind=kOutput, calls=%fused_computation | convolution fusion | flops 4306501632 | bytes 20979712 | tf_op jit(solution)/shard_map/dot_general | solution.py:89
  135.4 11.4 %reduce-scatter.3.cloned.1.call-done = bf16[128,2048]{1,0:T(8,128)(2,1)} async-done(((bf16[512,2048]{1,0:T(8,128)(2,1)}), bf16[128,2048]{1,0:T(8,128)(2,1)}) %reduce-scatter.3.cloned.1.call-update) | async-done | bytes 524304 | tf_op jit(solution)/shard_map/reduce_scatter | solution.py:68
  146.8 108.0 %reduce-scatter.5.cloned.1.call-done = bf16[128,2048]{1,0:T(8,128)(2,1)} async-done(((bf16[2048,2048]{1,0:T(8,128)(2,1)}), bf16[128,2048]{1,0:T(8,128)(2,1)}) %reduce-scatter.5.cloned.1.call-update) | async-done | bytes 524304 | tf_op jit(solution)/shard_map/reduce_scatter | solution.py:90
  (36 shorter events, 0.3 us)
Async XLA Ops:
  7.2 43.8 %copy-start = (bf16[512,2048]{1,0:T(8,128)(2,1)S(1)}, bf16[512,2048]{1,0:T(8,128)(2,1)}, u32[]{:S(2)}) copy-start(bf16[512,2048]{1,0:T(8,128)(2,1)} %param.18) | copy-start | bytes 6291460
  7.2 4.2 %copy-start.4 = (bf16[2048]{0:T(1024)(128)(2,1)S(1)}, bf16[2048]{0:T(1024)(128)(2,1)}, u32[]{:S(2)}) copy-start(bf16[2048]{0:T(1024)(128)(2,1)} %param.20) | copy-start | bytes 12292
  7.2 4.3 %copy-start.3 = (bf16[128,2048]{1,0:T(8,128)(2,1)S(1)}, bf16[128,2048]{1,0:T(8,128)(2,1)}, u32[]{:S(2)}) copy-start(bf16[128,2048]{1,0:T(8,128)(2,1)} %param.19) | copy-start | bytes 1572868
  7.2 29.6 %all-gather.3.cloned.1.call-start = ((), (), s32[]{:S(2)}) async-start(), calls=%async_computation.2 | async-start | bytes 2621440 | tf_op jit(solution)/shard_map/all_gather | solution.py:44
  11.4 102.6 %all-gather.5.cloned.1.call-start = ((), (), s32[]{:S(2)}) async-start(), calls=%async_computation.4 | async-start | bytes 8912896 | tf_op jit(solution)/shard_map/all_gather | solution.py:84
  12.7 134.2 %reduce-scatter.3.cloned.1.call-start = ((), (), s32[]{:S(2)}) async-start(), calls=%async_computation.3 | async-start | bytes 2621440 | tf_op jit(solution)/shard_map/reduce_scatter | solution.py:68
  12.7 32.0 %copy-start.6 = (bf16[512]{0:T(512)(128)(2,1)S(1)}, bf16[512]{0:T(512)(128)(2,1)}, u32[]{:S(2)}) copy-start(bf16[512]{0:T(512)(128)(2,1)} %param.17) | copy-start | bytes 3076
  41.3 3.4 %copy-start.8 = (bf16[512,512]{1,0:T(8,128)(2,1)}, bf16[512,512]{1,0:T(8,128)(2,1)S(1)}, u32[]{:S(2)}) copy-start(bf16[512,512]{1,0:T(8,128)(2,1)S(1)} %get-tuple-element.5) | copy-start | bytes 1572868
  41.3 4.8 %collective-permute-start = (bf16[16,512]{1,0:T(8,128)(2,1)S(1)}, bf16[16,512]{1,0:T(8,128)(2,1)S(1)}, u32[]{:S(2)}, u32[]{:S(2)}) collective-permute-start(bf16[16,512]{1,0:T(8,128)(2,1)S(1)} %slice.52), channel_id=1, source_target_pairs={{0,4},{4,8},{8,12},{1,5},{5,9},{9,13},{2,6},{6,10},{10,14},{3,7},{... | collective-permute-start | bytes 49160 | tf_op jit(solution)/shard_map/ppermute | solution.py:12
  48.2 1.0 copy-start.1
  49.3 1.6 copy-start.2
  56.8 0.7 copy-start.5
  56.8 0.7 copy-start.7
  56.8 57.2 %copy-start.9 = (bf16[1,2048,256]{2,1,0:T(8,128)(2,1)S(1)}, bf16[1,2048,256]{2,1,0:T(8,128)(2,1)}, u32[]{:S(2)}) copy-start(bf16[1,2048,256]{2,1,0:T(8,128)(2,1)} %param.23) | copy-start | bytes 3145732
  56.8 198.0 %reduce-scatter.5.cloned.1.call-start = ((), (), s32[]{:S(2)}) async-start(), calls=%async_computation.5 | async-start | bytes 8912896 | tf_op jit(solution)/shard_map/reduce_scatter | solution.py:90
Sparse Core Ops, SparseCore 0:
  11.5 25.2 all-gather.2
  39.5 74.3 all-gather.4
  117.1 29.7 reduce-scatter.2
  151.3 103.4 reduce-scatter.4

commit v2 on v0

--- a/solution.py
+++ b/solution.py
@@ -10,6 +10,13 @@
     devices = lax.axis_size(axis)
     pairs = [(i, i + by) for i in range(devices) if 0 <= i + by < devices]
     return lax.ppermute(value, axis, pairs)
+
+
+def turned(value, axis, by):
+    devices = lax.axis_size(axis)
+    if by % devices == 0:
+        return value
+    return lax.ppermute(value, axis, [(i, (i + by) % devices) for i in range(devices)])
 
 
 def rms_rows(rows, gain):
@@ -40,8 +47,23 @@
     down_weight,
 ):
     normed = rms_rows(mixer_tokens, mixer_gain)
+    expert_in = rms_rows(expert_tokens, expert_gain)
+    shares = route_weights / jnp.sum(route_weights, axis=1, keepdims=True)
+    rows_here, top_k = route_ids.shape
+    width = expert_in.shape[1]
+    n_experts = lax.axis_size("ep") * gate_weight.shape[0]
+    capacity = 4 * rows_here // n_experts
+    dense = capacity >= rows_here
+    parts_tp = lax.axis_size("tp")
+    if dense:
+        both = lax.all_gather(jnp.concatenate([normed, expert_in], axis=0), "tp", axis=0, tiled=True)
+        both = both.reshape(parts_tp, 2, rows_here, width)
+        every = both[:, 0].reshape(parts_tp * rows_here, width)
+        own = both[:, 1].reshape(parts_tp * rows_here, width)
+    else:
+        every = lax.all_gather(normed, "tp", axis=0, tiled=True)
     pooled_in = jnp.dot(
-        lax.all_gather(normed, "tp", axis=0, tiled=True),
+        every,
         in_weight,
         preferred_element_type=jnp.float32,
     ).astype(jnp.bfloat16)
@@ -64,19 +86,44 @@
         jnp.dot(pooled, group_weight[0], preferred_element_type=jnp.float32)
         * channel_scale.astype(jnp.float32)
     ).astype(jnp.bfloat16)
-    rows = grouped
-    mixed_tokens = lax.psum_scatter(
-        jnp.dot(rows, out_weight, preferred_element_type=jnp.float32).astype(jnp.bfloat16),
-        "tp",
-        scatter_dimension=0,
-        tiled=True,
+    mixed_part = jnp.dot(grouped, out_weight, preferred_element_type=jnp.float32).astype(
+        jnp.bfloat16
     )
-    expert_in = rms_rows(expert_tokens, expert_gain)
-    shares = route_weights / jnp.sum(route_weights, axis=1, keepdims=True)
-    rows_here, top_k = route_ids.shape
-    width = expert_in.shape[1]
-    n_experts = lax.axis_size("ep") * gate_weight.shape[0]
-    capacity = 4 * rows_here // n_experts
+    if dense:
+        experts = jnp.arange(n_experts, dtype=jnp.int32)
+        named = (route_ids[:, :, None] == experts[None, None, :]).astype(jnp.float32)
+        coefs = jnp.sum(named * shares[:, :, None], axis=1)
+        coefs = lax.all_gather(coefs, ("ep", "tp"), axis=0, tiled=True)
+        blocks = lax.axis_size("ep")
+        here = lax.axis_index("ep")
+        mine = (experts == here).astype(jnp.float32)
+        coef = jnp.sum(coefs * mine[None, :], axis=1).reshape(blocks, parts_tp, rows_here)
+        order = list(range(1, blocks))
+
+        def scale_of(k):
+            return lax.dynamic_index_in_dim(coef, lax.rem(here - k + blocks, blocks), 0, False)
+
+        def expert_part(rows, scale):
+            hidden = expert_hidden(rows, gate_weight[0], up_weight[0])
+            part = jnp.dot(hidden, down_weight[0], preferred_element_type=jnp.float32)
+            return (part * scale.reshape(-1)[:, None]).astype(jnp.bfloat16)
+
+        moved = jnp.concatenate([turned(expert_in, "ep", k) for k in order], axis=0)
+        moved, own = lax.optimization_barrier((moved, own))
+        own_part = expert_part(own, scale_of(0))
+        others = lax.all_gather(moved, "tp", axis=0, tiled=True)
+        part = expert_part(others, jnp.stack([scale_of(k) for k in order], axis=1))
+        back = lax.psum_scatter(part, "tp", scatter_dimension=0, tiled=True)
+        back = back.reshape(blocks - 1, rows_here, width)
+        pair = jnp.stack(
+            [value.reshape(parts_tp, rows_here, width) for value in (mixed_part, own_part)], axis=1
+        ).reshape(2 * parts_tp * rows_here, width)
+        pair = lax.psum_scatter(pair, "tp", scatter_dimension=0, tiled=True)
+        total = pair[rows_here:].astype(jnp.float32)
+        for i, k in enumerate(order):
+            total = total + turned(back[i], "ep", -k).astype(jnp.float32)
+        return (pair[:rows_here], total.astype(jnp.bfloat16))
+    mixed_tokens = lax.psum_scatter(mixed_part, "tp", scatter_dimension=0, tiled=True)
     flat_ids = route_ids.reshape(rows_here * top_k)
     one_hot = (flat_ids[:, None] == jnp.arange(n_experts, dtype=jnp.int32)[None, :]).astype(
         jnp.int32

time: 306 us -> 253 us (0.83)
  waiting for transfers between devices: 157 us -> 126 us
  blocking collectives: 54.4 us -> 31.1 us
  starting transfers between devices: 8.52 us -> 15.1 us
  other arithmetic: 18.3 us -> 15.2 us
    all_to_all x1 -> x0, blocking collectives: 54.4 us -> none  [local(): lax.all_to_all(outgoing, 'ep', split_axis=0, concat_axis=0, tiled=True)]
    all_to_all x1 -> x0, waiting for transfers between devices: 47.6 us -> none  [local(): lax.all_to_all(summed.reshape(sources, held, width).astype(jnp.bfloat16),...]
    ppermute x0 -> x6, waiting for transfers between devices: none -> 34.6 us  [turned(): lax.ppermute(value, axis, [(i, (i + by) % devices) for i in range(devices)])]
    all_gather x0 -> x1, blocking collectives: none -> 31.1 us  [local(): coefs = lax.all_gather(coefs, ('ep', 'tp'), axis=0, tiled=True)]
    all_gather x2, waiting for transfers between devices: 55.4 us -> 25.6 us  [the longest x1 25.6 us: local(): others = lax.all_gather(moved, 'tp', axis=0, tiled=True)]
    reduce_scatter x2, waiting for transfers between devices: 52.4 us -> 66 us  [the longest x1 40 us: local(): pair = lax.psum_scatter(pair, 'tp', scatter_dimension=0, tiled=True)]
    ppermute x0 -> x6, starting transfers between devices: none -> 11.5 us  [turned(): lax.ppermute(value, axis, [(i, (i + by) % devices) for i in range(devices)])]
    gather x2 -> x0, local copies, waits for them, and re-layouts: 9.3 us -> none  [local(): jnp.take(flat_out, targets, axis=0).reshape(rows_here, top_k, width)]
  transfers between devices with their start and end apart: 6 -> 11, of which waited for: 4 -> 6; matrix products, arithmetic and copies ran while one was open for 20% -> 13% of each run, Pallas kernels for 0% -> 0%
where the time goes in v2:
time: 253 us; the launch traced here: 252 us
  waiting for transfers between devices  126 us (50%)
  matrix products  35.7 us (14%)
  blocking collectives  31.1 us (12%)
  other arithmetic  15.2 us (6%)
  starting transfers between devices  15.1 us (6%)
  local copies, waits for them, and re-layouts  15 us (6%)
  between operations  14 us (6%)
    reduce_scatter x1, waiting for transfers between devices, local(): pair = lax.psum_scatter(pair, 'tp', scatter_dimension=0, tiled=True)  40 us
    ppermute x6, waiting for transfers between devices, turned(): lax.ppermute(value, axis, [(i, (i + by) % devices) for i in range(devices)])  34.6 us
    all_gather x1, blocking collectives, local(): coefs = lax.all_gather(coefs, ('ep', 'tp'), axis=0, tiled=True)  31.1 us
    reduce_scatter x1, waiting for transfers between devices, local(): back = lax.psum_scatter(part, 'tp', scatter_dimension=0, tiled=True)  25.9 us
    all_gather x1, waiting for transfers between devices, local(): others = lax.all_gather(moved, 'tp', axis=0, tiled=True)  25.6 us
    dot_general x2, matrix products, expert_part(): part = jnp.dot(hidden, down_weight[0], preferred_element_type=jnp.float32)  17.5 us
    ppermute x6, starting transfers between devices, turned(): lax.ppermute(value, axis, [(i, (i + by) % devices) for i in range(devices)])  11.5 us
    dot_general x2, matrix products, expert_hidden(): gate = jnp.dot(rows, w_gate, preferred_element_type=jnp.float32)  7.27 us
  transfers between devices with their start and end apart: 11, of which 6 were waited for; matrix products, arithmetic and copies ran while one was open for 13% of the time, Pallas kernels for 0%

profile of v2, /device:TPU:0, one launch (start us, length us, event | category | flops | bytes accessed | tf_op | source)
XLA Modules:
  0.0 252.4 jit_solution(7683948165691868259)
XLA Ops:
  13.9 3.1 %collective-permute-start.1 = (bf16[128,2048]{1,0:T(8,128)(2,1)S(1)}, bf16[128,2048]{1,0:T(8,128)(2,1)S(1)}, u32[]{:S(2)}, u32[]{:S(2)}) collective-permute-start(bf16[128,2048]{1,0:T(8,128)(2,1)S(1)} %get-tuple-element.20), channel_id=1, source_target_pairs={{0,4},{4,8},{8,12},{12,0},{1,5},{5,9},{9,13},{13,1},{2,6},{6,10},{... | collective-permute-start | bytes 1572872 | tf_op jit(solution)/shard_map/ppermute | solution.py:19
  17.0 2.6 %collective-permute-start.2 = (bf16[128,2048]{1,0:T(8,128)(2,1)S(1)}, bf16[128,2048]{1,0:T(8,128)(2,1)S(1)}, u32[]{:S(2)}, u32[]{:S(2)}) collective-permute-start(bf16[128,2048]{1,0:T(8,128)(2,1)S(1)} %get-tuple-element.20), channel_id=1, source_target_pairs={{0,8},{4,12},{8,0},{12,4},{1,9},{5,13},{9,1},{13,5},{2,10},{6,14},... | collective-permute-start | bytes 1572872 | tf_op jit(solution)/shard_map/ppermute | solution.py:19
  20.9 11.0 %collective-permute-done.1 = bf16[128,2048]{1,0:T(8,128)(2,1)S(1)} collective-permute-done((bf16[128,2048]{1,0:T(8,128)(2,1)S(1)}, bf16[128,2048]{1,0:T(8,128)(2,1)S(1)}, u32[]{:S(2)}, u32[]{:S(2)}) %collective-permute-start.1) | collective-permute-done | bytes 524320 | tf_op jit(solution)/shard_map/ppermute | solution.py:19
  31.9 21.6 %collective-permute-done.2 = bf16[128,2048]{1,0:T(8,128)(2,1)S(1)} collective-permute-done((bf16[128,2048]{1,0:T(8,128)(2,1)S(1)}, bf16[128,2048]{1,0:T(8,128)(2,1)S(1)}, u32[]{:S(2)}, u32[]{:S(2)}) %collective-permute-start.2) | collective-permute-done | bytes 524320 | tf_op jit(solution)/shard_map/ppermute | solution.py:19
  54.9 4.9 %fusion.57 = (bf16[4,1,128,2048]{3,2,1,0:T(8,128)(2,1)}, bf16[4,1,128,2048]{3,2,1,0:T(8,128)(2,1)}) fusion(bf16[4,2,128,2048]{3,2,1,0:T(8,128)(2,1)} %bitcast.41), kind=kLoop, calls=%fused_computation.79 | loop fusion | bytes 8388608 | tf_op jit(solution)/shard_map/slice | solution.py:61
  59.9 31.1 %all_gather.10 = f32[2048,4]{0,1:T(4,128)S(1)} all-gather(f32[128,4]{0,1:T(4,128)S(1)} %select_reduce_fusion), channel_id=1, replica_groups=mesh['grp'=2,'ep'=4,'tp'=4] {'ep','tp'}, dimensions={0}, use_global_device_ids=true | all-gather | bytes 34816 | tf_op jit(solution)/shard_map/all_gather | solution.py:96
  91.2 25.6 %all-gather.5.cloned.1.call-done = bf16[1536,2048]{1,0:T(8,128)(2,1)} async-done(((bf16[384,2048]{1,0:T(8,128)(2,1)}), bf16[1536,2048]{1,0:T(8,128)(2,1)}) %all-gather.5.cloned.1.call-update) | async-done | bytes 6291472 | tf_op jit(solution)/shard_map/all_gather | solution.py:114
  116.8 5.8 %fusion.22 = f32[1536,256]{1,0:T(8,128)} fusion(bf16[1536,2048]{1,0:T(8,128)(2,1)} %all-gather.5.cloned.1.call-done, bf16[1,2048,256]{2,1,0:T(8,128)(2,1)S(1)} %copy-done.8), kind=kOutput, calls=%fused_computation.41 | convolution fusion | flops 1610612736 | bytes 8912896 | tf_op jit(solution)/shard_map/dot_general | solution.py:29
  122.5 11.1 %multiply_convert_fusion = bf16[1536,2048]{1,0:T(8,128)(2,1)} fusion(f32[1536]{0:T(1024)S(1)} %mul.123, bf16[1536,2048]{1,0:T(8,128)(2,1)} %all-gather.5.cloned.1.call-done, f32[1536,256]{1,0:T(8,128)} %fusion.22, bf16[1,256,2048]{2,1,0:T(8,128)(2,1)} %param.25, bf16[1,2048,256]{2,1,0:T(8,128)(2,1)} %param.24), kind=kOutput, calls=%fused_computation | convolution fusion | flops 3229876224 | bytes 16259072 | tf_op jit(solution)/shard_map/dot_general | solution.py:108
  134.3 4.7 %fusion.60 = (f32[512,512]{1,0:T(8,128)}, bf16[512,512]{1,0:T(8,128)(2,1)S(1)}) fusion(bf16[512,2048]{1,0:T(8,128)(2,1)} %bitcast.44, bf16[2048,512]{1,0:T(8,128)(2,1)} %param.15), kind=kOutput, calls=%fused_computation.82 | convolution fusion | flops 1074266112 | bytes 5767168 | tf_op jit(solution)/shard_map/dot_general | solution.py:65
  139.0 3.5 %collective-permute-start = (bf16[16,512]{1,0:T(8,128)(2,1)S(1)}, bf16[16,512]{1,0:T(8,128)(2,1)S(1)}, u32[]{:S(2)}, u32[]{:S(2)}) collective-permute-start(bf16[16,512]{1,0:T(8,128)(2,1)S(1)} %slice.84), channel_id=1, source_target_pairs={{0,4},{4,8},{8,12},{1,5},{5,9},{9,13},{2,6},{6,10},{10,14},{3,7},{... | collective-permute-start | bytes 49160 | tf_op jit(solution)/shard_map/ppermute | solution.py:12
  144.1 6.4 %multiply_convert_fusion.1 = bf16[512,2048]{1,0:T(8,128)(2,1)} fusion(f32[512]{0:T(512)S(1)} %get-tuple-element.16, bf16[512,2048]{1,0:T(8,128)(2,1)} %bitcast.42, bf16[1,256,2048]{2,1,0:T(8,128)(2,1)} %param.25, bf16[1,2048,256]{2,1,0:T(8,128)(2,1)} %param.24, f32[512,256]{1,0:T(8,128)} %fusion.24), kind=kOutput, calls=%fused_computation.2 | convolution fusion | flops 1076625408 | bytes 6817792 | tf_op jit(solution)/shard_map/dot_general | solution.py:108
  150.5 1.9 fusion.3
  153.7 1.7 fusion.59
  155.4 6.3 %convolution_convert_fusion = bf16[512,2048]{1,0:T(8,128)(2,1)} fusion(bf16[512,2048]{1,0:T(8,128)(2,1)S(1)} %copy-done, f32[513,512]{1,0:T(8,128)} %get-tuple-element.12, f32[513,512]{1,0:T(8,128)} %get-tuple-element.11, f32[521,512]{1,0:T(8,128)} %copy-done.2, f32[525,512]{1,0:T(8,128)} %copy-done.1, f32[527,512]{1,0:T(8,128)S(1)} %fusion.3, ...), kind=kOutput, calls=%fused_computation.3 | convolution fusion | flops 1346895872 | bytes 10489860 | tf_op jit(solution)/shard_map/dot_general | solution.py:89
  161.7 2.6 %pad_maximum_fusion = bf16[4,2,128,2048]{3,2,0,1:T(8,128)(2,1)S(1)} fusion(bf16[4,1,128,2048]{3,2,0,1:T(8,128)(2,1)} %bitcast.45, bf16[4,1,128,2048]{3,2,0,1:T(8,128)(2,1)} %bitcast.46), kind=kLoop, calls=%fused_computation.1 | loop fusion | flops 2097152 | bytes 8388608 | tf_op jit(solution)/shard_map/stack | solution.py:118
  164.3 2.3 copy.21
  166.7 25.9 %reduce-scatter.5.cloned.1.call-done = bf16[384,2048]{1,0:T(8,128)(2,1)} async-done(((bf16[1536,2048]{1,0:T(8,128)(2,1)}), bf16[384,2048]{1,0:T(8,128)(2,1)}) %reduce-scatter.5.cloned.1.call-update) | async-done | bytes 1572880 | tf_op jit(solution)/shard_map/reduce_scatter | solution.py:116
  192.6 2.6 %fusion.58 = (bf16[128,2048]{1,0:T(8,128)(2,1)}, bf16[128,2048]{1,0:T(8,128)(2,1)}, bf16[128,2048]{1,0:T(8,128)(2,1)}) fusion(bf16[384,2048]{1,0:T(8,128)(2,1)} %reduce-scatter.5.cloned.1.call-done), kind=kLoop, calls=%fused_computation.80 | loop fusion | bytes 3145728 | tf_op jit(solution)/shard_map/slice | solution.py:124
  195.2 3.3 %collective-permute-start.4 = (bf16[128,2048]{1,0:T(8,128)(2,1)}, bf16[128,2048]{1,0:T(8,128)(2,1)S(1)}, u32[]{:S(2)}, u32[]{:S(2)}) collective-permute-start(bf16[128,2048]{1,0:T(8,128)(2,1)} %get-tuple-element.8), channel_id=1, source_target_pairs={{0,12},{4,0},{8,4},{12,8},{1,13},{5,1},{9,5},{13,9},{2,14},{6,2},{... | collective-permute-start | bytes 1572872 | tf_op jit(solution)/shard_map/ppermute | solution.py:19
  199.6 40.0 %reduce-scatter.3.cloned.1.call-done = bf16[256,2048]{1,0:T(8,128)(2,1)} async-done(((bf16[1024,2048]{1,0:T(8,128)(2,1)}), bf16[256,2048]{1,0:T(8,128)(2,1)}) %reduce-scatter.3.cloned.1.call-update) | async-done | bytes 1048592 | tf_op jit(solution)/shard_map/reduce_scatter | solution.py:121
  239.6 1.9 slice.99
  241.5 2.0 collective-permute-done.5
  243.5 2.3 add_convert_fusion
  (60 shorter events, 14.2 us)
Async XLA Ops:
  7.2 148.3 %copy-start = (bf16[512,2048]{1,0:T(8,128)(2,1)S(1)}, bf16[512,2048]{1,0:T(8,128)(2,1)}, u32[]{:S(2)}) copy-start(bf16[512,2048]{1,0:T(8,128)(2,1)} %param.18) | copy-start | bytes 6291460
  7.2 47.7 %all-gather.3.cloned.1.call-start = ((), (), s32[]{:S(2)}) async-start(), calls=%async_computation.2 | async-start | bytes 5242880 | tf_op jit(solution)/shard_map/all_gather | solution.py:59
  13.8 102.9 %all-gather.5.cloned.1.call-start = ((), (), s32[]{:S(2)}) async-start(), calls=%async_computation.4 | async-start | bytes 7864320 | tf_op jit(solution)/shard_map/all_gather | solution.py:114
  13.9 18.0 %collective-permute-start.1 = (bf16[128,2048]{1,0:T(8,128)(2,1)S(1)}, bf16[128,2048]{1,0:T(8,128)(2,1)S(1)}, u32[]{:S(2)}, u32[]{:S(2)}) collective-permute-start(bf16[128,2048]{1,0:T(8,128)(2,1)S(1)} %get-tuple-element.20), channel_id=1, source_target_pairs={{0,4},{4,8},{8,12},{12,0},{1,5},{5,9},{9,13},{13,1},{2,6},{6,10},{... | collective-permute-start | bytes 1572872 | tf_op jit(solution)/shard_map/ppermute | solution.py:19
  17.0 36.6 %collective-permute-start.2 = (bf16[128,2048]{1,0:T(8,128)(2,1)S(1)}, bf16[128,2048]{1,0:T(8,128)(2,1)S(1)}, u32[]{:S(2)}, u32[]{:S(2)}) collective-permute-start(bf16[128,2048]{1,0:T(8,128)(2,1)S(1)} %get-tuple-element.20), channel_id=1, source_target_pairs={{0,8},{4,12},{8,0},{12,4},{1,9},{5,13},{9,1},{13,5},{2,10},{6,14},... | collective-permute-start | bytes 1572872 | tf_op jit(solution)/shard_map/ppermute | solution.py:19
  19.6 34.0 %collective-permute-start.3 = (bf16[128,2048]{1,0:T(8,128)(2,1)S(1)}, bf16[128,2048]{1,0:T(8,128)(2,1)S(1)}, u32[]{:S(2)}, u32[]{:S(2)}) collective-permute-start(bf16[128,2048]{1,0:T(8,128)(2,1)S(1)} %get-tuple-element.20), channel_id=1, source_target_pairs={{0,12},{4,0},{8,4},{12,8},{1,13},{5,1},{9,5},{13,9},{2,14},{6,2},{... | collective-permute-start | bytes 1572872 | tf_op jit(solution)/shard_map/ppermute | solution.py:19
  54.8 5.0 %copy-start.4 = (f32[128,2]{0,1:T(2,128)S(1)}, f32[128,2]{0,1:T(2,128)}, u32[]{:S(2)}) copy-start(f32[128,2]{0,1:T(2,128)} %param.22) | copy-start | bytes 3076
  54.8 5.0 %copy-start.6 = (s32[128,2]{0,1:T(2,128)S(1)}, s32[128,2]{0,1:T(2,128)}, u32[]{:S(2)}) copy-start(s32[128,2]{0,1:T(2,128)} %param.21) | copy-start | bytes 3076
  54.8 61.9 %copy-start.8 = (bf16[1,2048,256]{2,1,0:T(8,128)(2,1)S(1)}, bf16[1,2048,256]{2,1,0:T(8,128)(2,1)}, u32[]{:S(2)}) copy-start(bf16[1,2048,256]{2,1,0:T(8,128)(2,1)} %param.23) | copy-start | bytes 3145732
  59.8 132.9 %reduce-scatter.5.cloned.1.call-start = ((), (), s32[]{:S(2)}) async-start(), calls=%async_computation.5 | async-start | bytes 7864320 | tf_op jit(solution)/shard_map/reduce_scatter | solution.py:116
  133.6 0.7 copy-start.5
  133.7 106.0 %reduce-scatter.3.cloned.1.call-start = ((), (), s32[]{:S(2)}) async-start(), calls=%async_computation.3 | async-start | bytes 5242880 | tf_op jit(solution)/shard_map/reduce_scatter | solution.py:121
  134.3 8.2 %copy-start.3 = (bf16[4,1,128,2048]{3,2,1,0:T(8,128)(2,1)S(1)}, bf16[4,1,128,2048]{3,2,1,0:T(8,128)(2,1)}, u32[]{:S(2)}) copy-start(bf16[4,1,128,2048]{3,2,1,0:T(8,128)(2,1)} %get-tuple-element.7) | copy-start | bytes 6291460
  134.3 8.2 %copy-start.9 = (bf16[1,2048,256]{2,1,0:T(8,128)(2,1)S(1)}, bf16[1,2048,256]{2,1,0:T(8,128)(2,1)}, u32[]{:S(2)}) copy-start(bf16[1,2048,256]{2,1,0:T(8,128)(2,1)} %param.23) | copy-start | bytes 3145732
  139.0 11.5 %copy-start.7 = (bf16[512,512]{1,0:T(8,128)(2,1)}, bf16[512,512]{1,0:T(8,128)(2,1)S(1)}, u32[]{:S(2)}) copy-start(bf16[512,512]{1,0:T(8,128)(2,1)S(1)} %get-tuple-element.18) | copy-start | bytes 1572868
  139.0 11.4 %collective-permute-start = (bf16[16,512]{1,0:T(8,128)(2,1)S(1)}, bf16[16,512]{1,0:T(8,128)(2,1)S(1)}, u32[]{:S(2)}, u32[]{:S(2)}) collective-permute-start(bf16[16,512]{1,0:T(8,128)(2,1)S(1)} %slice.84), channel_id=1, source_target_pairs={{0,4},{4,8},{8,12},{1,5},{5,9},{9,13},{2,6},{6,10},{10,14},{3,7},{... | collective-permute-start | bytes 49160 | tf_op jit(solution)/shard_map/ppermute | solution.py:12
  152.6 1.0 copy-start.1
  153.7 1.7 copy-start.2
  195.2 46.3 %collective-permute-start.4 = (bf16[128,2048]{1,0:T(8,128)(2,1)}, bf16[128,2048]{1,0:T(8,128)(2,1)S(1)}, u32[]{:S(2)}, u32[]{:S(2)}) collective-permute-start(bf16[128,2048]{1,0:T(8,128)(2,1)} %get-tuple-element.8), channel_id=1, source_target_pairs={{0,12},{4,0},{8,4},{12,8},{1,13},{5,1},{9,5},{13,9},{2,14},{6,2},{... | collective-permute-start | bytes 1572872 | tf_op jit(solution)/shard_map/ppermute | solution.py:19
  198.5 45.0 %collective-permute-start.5 = (bf16[128,2048]{1,0:T(8,128)(2,1)}, bf16[128,2048]{1,0:T(8,128)(2,1)S(1)}, u32[]{:S(2)}, u32[]{:S(2)}) collective-permute-start(bf16[128,2048]{1,0:T(8,128)(2,1)} %get-tuple-element.10), channel_id=1, source_target_pairs={{0,8},{4,12},{8,0},{12,4},{1,9},{5,13},{9,1},{13,5},{2,10},{6,14},... | collective-permute-start | bytes 1572872 | tf_op jit(solution)/shard_map/ppermute | solution.py:19
  198.5 45.0 %collective-permute-start.6 = (bf16[128,2048]{1,0:T(8,128)(2,1)}, bf16[128,2048]{1,0:T(8,128)(2,1)}, u32[]{:S(2)}, u32[]{:S(2)}) collective-permute-start(bf16[128,2048]{1,0:T(8,128)(2,1)} %get-tuple-element.9), channel_id=1, source_target_pairs={{0,4},{4,8},{8,12},{12,0},{1,5},{5,9},{9,13},{13,1},{2,6},{6,10},{... | collective-permute-start | bytes 1572872 | tf_op jit(solution)/shard_map/ppermute | solution.py:19
Sparse Core Ops, SparseCore 0:
  14.0 37.1 all-gather.2
  59.9 56.8 all-gather.4
  133.8 58.8 reduce-scatter.4
  195.0 44.5 reduce-scatter.2

commit v3 on v2

--- a/solution.py
+++ b/solution.py
@@ -55,13 +55,10 @@
     capacity = 4 * rows_here // n_experts
     dense = capacity >= rows_here
     parts_tp = lax.axis_size("tp")
+    every = lax.all_gather(normed, "tp", axis=0, tiled=True)
     if dense:
-        both = lax.all_gather(jnp.concatenate([normed, expert_in], axis=0), "tp", axis=0, tiled=True)
-        both = both.reshape(parts_tp, 2, rows_here, width)
-        every = both[:, 0].reshape(parts_tp * rows_here, width)
-        own = both[:, 1].reshape(parts_tp * rows_here, width)
-    else:
-        every = lax.all_gather(normed, "tp", axis=0, tiled=True)
+        moved = [turned(expert_in, "ep", k) for k in range(lax.axis_size("ep"))]
+        moved, every = lax.optimization_barrier((jnp.concatenate(moved, axis=0), every))
     pooled_in = jnp.dot(
         every,
         in_weight,
@@ -98,7 +95,7 @@
         here = lax.axis_index("ep")
         mine = (experts == here).astype(jnp.float32)
         coef = jnp.sum(coefs * mine[None, :], axis=1).reshape(blocks, parts_tp, rows_here)
-        order = list(range(1, blocks))
+        order = list(range(blocks))
 
         def scale_of(k):
             return lax.dynamic_index_in_dim(coef, lax.rem(here - k + blocks, blocks), 0, False)
@@ -108,21 +105,16 @@
             part = jnp.dot(hidden, down_weight[0], preferred_element_type=jnp.float32)
             return (part * scale.reshape(-1)[:, None]).astype(jnp.bfloat16)
 
-        moved = jnp.concatenate([turned(expert_in, "ep", k) for k in order], axis=0)
-        moved, own = lax.optimization_barrier((moved, own))
-        own_part = expert_part(own, scale_of(0))
         others = lax.all_gather(moved, "tp", axis=0, tiled=True)
         part = expert_part(others, jnp.stack([scale_of(k) for k in order], axis=1))
         back = lax.psum_scatter(part, "tp", scatter_dimension=0, tiled=True)
-        back = back.reshape(blocks - 1, rows_here, width)
-        pair = jnp.stack(
-            [value.reshape(parts_tp, rows_here, width) for value in (mixed_part, own_part)], axis=1
-        ).reshape(2 * parts_tp * rows_here, width)
-        pair = lax.psum_scatter(pair, "tp", scatter_dimension=0, tiled=True)
-        total = pair[rows_here:].astype(jnp.float32)
+        mixed_part, back = lax.optimization_barrier((mixed_part, back))
+        back = back.reshape(blocks, rows_here, width)
+        total = jnp.zeros((rows_here, width), jnp.float32)
         for i, k in enumerate(order):
             total = total + turned(back[i], "ep", -k).astype(jnp.float32)
-        return (pair[:rows_here], total.astype(jnp.bfloat16))
+        mixed_tokens = lax.psum_scatter(mixed_part, "tp", scatter_dimension=0, tiled=True)
+        return (mixed_tokens, total.astype(jnp.bfloat16))
     mixed_tokens = lax.psum_scatter(mixed_part, "tp", scatter_dimension=0, tiled=True)
     flat_ids = route_ids.reshape(rows_here * top_k)
     one_hot = (flat_ids[:, None] == jnp.arange(n_experts, dtype=jnp.int32)[None, :]).astype(

time: 253 us -> 272 us (1.075)
  the two profiles are of different devices: /device:TPU:0 before, /device:TPU:9 now
where the time goes in v3:
time: 272 us
  waiting for transfers between devices  181 us (67%)
  matrix products  31.4 us (12%)
  blocking collectives  18.3 us (7%)
  between operations  14 us (5%)
  starting transfers between devices  11.6 us (4%)
  other arithmetic  11 us (4%)
  local copies, waits for them, and re-layouts  4.87 us (2%)
    ppermute x6, waiting for transfers between devices, turned(): lax.ppermute(value, axis, [(i, (i + by) % devices) for i in range(devices)])  87.4 us
    reduce_scatter x1, waiting for transfers between devices, local(): back = lax.psum_scatter(part, 'tp', scatter_dimension=0, tiled=True)  50.5 us
    all_gather x1, waiting for transfers between devices, local(): others = lax.all_gather(moved, 'tp', axis=0, tiled=True)  41.3 us
    all_gather x1, blocking collectives, local(): coefs = lax.all_gather(coefs, ('ep', 'tp'), axis=0, tiled=True)  18.3 us
    dot_general x1, matrix products, expert_part(): part = jnp.dot(hidden, down_weight[0], preferred_element_type=jnp.float32)  13.8 us
    ppermute x6, starting transfers between devices, turned(): lax.ppermute(value, axis, [(i, (i + by) % devices) for i in range(devices)])  8.35 us
    dot_general x1, matrix products, expert_hidden(): gate = jnp.dot(rows, w_gate, preferred_element_type=jnp.float32)  7.05 us
    dot_general x1, matrix products, local(): jnp.dot(grouped, out_weight, preferred_element_type=jnp.float32)  6.09 us
  transfers between devices with their start and end apart: 11, of which 9 were waited for; matrix products, arithmetic and copies ran while one was open for 8% of the time, Pallas kernels for 0%

profile of v3, /device:TPU:9, one launch (start us, length us, event | category | flops | bytes accessed | tf_op | source)
XLA Modules:
  0.0 271.8 jit_solution(5121181731115763859)
XLA Ops:
  9.3 2.0 fusion.8
  11.9 2.5 collective-permute-start.1
  14.4 2.2 collective-permute-start
  16.6 8.2 %collective-permute-done.2 = bf16[128,2048]{1,0:T(8,128)(2,1)S(1)} collective-permute-done((bf16[128,2048]{1,0:T(8,128)(2,1)S(1)}, bf16[128,2048]{1,0:T(8,128)(2,1)S(1)}, u32[]{:S(2)}, u32[]{:S(2)}) %collective-permute-start.2) | collective-permute-done | bytes 524320 | tf_op jit(solution)/shard_map/ppermute | solution.py:19
  24.8 23.0 %collective-permute-done.1 = bf16[128,2048]{1,0:T(8,128)(2,1)S(1)} collective-permute-done((bf16[128,2048]{1,0:T(8,128)(2,1)S(1)}, bf16[128,2048]{1,0:T(8,128)(2,1)S(1)}, u32[]{:S(2)}, u32[]{:S(2)}) %collective-permute-start.1) | collective-permute-done | bytes 524320 | tf_op jit(solution)/shard_map/ppermute | solution.py:19
  47.8 11.2 %collective-permute-done = bf16[128,2048]{1,0:T(8,128)(2,1)S(1)} collective-permute-done((bf16[128,2048]{1,0:T(8,128)(2,1)S(1)}, bf16[128,2048]{1,0:T(8,128)(2,1)S(1)}, u32[]{:S(2)}, u32[]{:S(2)}) %collective-permute-start) | collective-permute-done | bytes 524320 | tf_op jit(solution)/shard_map/ppermute | solution.py:19
  59.1 1.6 pad_maximum_fusion
  61.4 18.3 %all_gather.11 = f32[2048,4]{0,1:T(4,128)S(1)} all-gather(f32[128,4]{0,1:T(4,128)S(1)} %select_reduce_fusion), channel_id=1, replica_groups=mesh['grp'=2,'ep'=4,'tp'=4] {'ep','tp'}, dimensions={0}, use_global_device_ids=true | all-gather | bytes 34816 | tf_op jit(solution)/shard_map/all_gather | solution.py:93
  79.8 41.3 %all-gather.5.cloned.1.call-done = bf16[2048,2048]{1,0:T(8,128)(2,1)} async-done(((bf16[512,2048]{1,0:T(8,128)(2,1)}), bf16[2048,2048]{1,0:T(8,128)(2,1)}) %all-gather.5.cloned.1.call-update) | async-done | bytes 8388624 | tf_op jit(solution)/shard_map/all_gather | solution.py:108
  121.2 7.1 %fusion.18 = f32[2048,256]{1,0:T(8,128)} fusion(bf16[2048,2048]{1,0:T(8,128)(2,1)} %all-gather.5.cloned.1.call-done, bf16[1,2048,256]{2,1,0:T(8,128)(2,1)S(1)} %copy-done.9), kind=kOutput, calls=%fused_computation.34 | convolution fusion | flops 2147483648 | bytes 11534336 | tf_op jit(solution)/shard_map/dot_general | solution.py:29
  128.2 13.8 %multiply_convert_fusion = bf16[2048,2048]{1,0:T(8,128)(2,1)} fusion(f32[2048]{0:T(1024)S(1)} %bitcast.26, bf16[2048,2048]{1,0:T(8,128)(2,1)} %all-gather.5.cloned.1.call-done, f32[2048,256]{1,0:T(8,128)} %fusion.18, bf16[1,256,2048]{2,1,0:T(8,128)(2,1)} %param.25, bf16[1,2048,256]{2,1,0:T(8,128)(2,1)} %param.24), kind=kOutput, calls=%fused_computation | convolution fusion | flops 4306501632 | bytes 20979712 | tf_op jit(solution)/shard_map/dot_general | solution.py:105
  142.1 4.5 %fusion.46 = (f32[512,512]{1,0:T(8,128)}, bf16[512,512]{1,0:T(8,128)(2,1)S(1)}) fusion(bf16[512,2048]{1,0:T(8,128)(2,1)} %all-gather.3.cloned.1.call-done, bf16[2048,512]{1,0:T(8,128)(2,1)} %param.15), kind=kOutput, calls=%fused_computation.65 | convolution fusion | flops 1074266112 | bytes 5767168 | tf_op jit(solution)/shard_map/dot_general | solution.py:62
  146.6 3.1 %collective-permute-start.3 = (bf16[16,512]{1,0:T(8,128)(2,1)S(1)}, bf16[16,512]{1,0:T(8,128)(2,1)S(1)}, u32[]{:S(2)}, u32[]{:S(2)}) collective-permute-start(bf16[16,512]{1,0:T(8,128)(2,1)S(1)} %slice.72), channel_id=1, source_target_pairs={{0,4},{4,8},{8,12},{1,5},{5,9},{9,13},{2,6},{6,10},{10,14},{3,7},{... | collective-permute-start | bytes 49160 | tf_op jit(solution)/shard_map/ppermute | solution.py:12
  149.8 1.3 collective-permute-done.3
  151.1 2.4 fusion.2
  154.7 1.7 fusion.45
  156.5 6.1 %convolution_convert_fusion = bf16[512,2048]{1,0:T(8,128)(2,1)} fusion(bf16[512,2048]{1,0:T(8,128)(2,1)S(1)} %copy-done, f32[513,512]{1,0:T(8,128)} %get-tuple-element.14, f32[513,512]{1,0:T(8,128)} %get-tuple-element.13, f32[521,512]{1,0:T(8,128)} %copy-done.2, f32[525,512]{1,0:T(8,128)} %copy-done.1, f32[527,512]{1,0:T(8,128)S(1)} %fusion.2, ...), kind=kOutput, calls=%fused_computation.1 | convolution fusion | flops 1346895872 | bytes 10489860 | tf_op jit(solution)/shard_map/dot_general | solution.py:86
  162.6 50.5 %reduce-scatter.3.cloned.1.call-done = bf16[512,2048]{1,0:T(8,128)(2,1)} async-done(((bf16[2048,2048]{1,0:T(8,128)(2,1)}), bf16[512,2048]{1,0:T(8,128)(2,1)}) %reduce-scatter.3.cloned.1.call-update) | async-done | bytes 2097168 | tf_op jit(solution)/shard_map/reduce_scatter | solution.py:110
  213.1 1.5 fusion.44
  214.6 1.3 collective-permute-start.6
  218.2 9.1 %collective-permute-done.6 = bf16[128,2048]{1,0:T(8,128)(2,1)S(1)} collective-permute-done((bf16[128,2048]{1,0:T(8,128)(2,1)S(1)}, bf16[128,2048]{1,0:T(8,128)(2,1)S(1)}, u32[]{:S(2)}, u32[]{:S(2)}) %collective-permute-start.6) | collective-permute-done | bytes 524320 | tf_op jit(solution)/shard_map/ppermute | solution.py:19
  227.3 32.7 %collective-permute-done.5 = bf16[128,2048]{1,0:T(8,128)(2,1)S(1)} collective-permute-done((bf16[128,2048]{1,0:T(8,128)(2,1)S(1)}, bf16[128,2048]{1,0:T(8,128)(2,1)S(1)}, u32[]{:S(2)}, u32[]{:S(2)}) %collective-permute-start.5) | collective-permute-done | bytes 524320 | tf_op jit(solution)/shard_map/ppermute | solution.py:19
  260.0 3.1 %collective-permute-done.4 = bf16[128,2048]{1,0:T(8,128)(2,1)S(1)} collective-permute-done((bf16[128,2048]{1,0:T(8,128)(2,1)S(1)}, bf16[128,2048]{1,0:T(8,128)(2,1)S(1)}, u32[]{:S(2)}, u32[]{:S(2)}) %collective-permute-start.4) | collective-permute-done | bytes 524320 | tf_op jit(solution)/shard_map/ppermute | solution.py:19
  263.1 2.2 add_convert_fusion
  (53 shorter events, 7.2 us)
Async XLA Ops:
  7.2 149.3 %copy-start = (bf16[512,2048]{1,0:T(8,128)(2,1)S(1)}, bf16[512,2048]{1,0:T(8,128)(2,1)}, u32[]{:S(2)}) copy-start(bf16[512,2048]{1,0:T(8,128)(2,1)} %param.18) | copy-start | bytes 6291460
  7.2 4.2 %copy-start.4 = (bf16[2048]{0:T(1024)(128)(2,1)S(1)}, bf16[2048]{0:T(1024)(128)(2,1)}, u32[]{:S(2)}) copy-start(bf16[2048]{0:T(1024)(128)(2,1)} %param.20) | copy-start | bytes 12292
  7.2 4.3 %copy-start.3 = (bf16[128,2048]{1,0:T(8,128)(2,1)S(1)}, bf16[128,2048]{1,0:T(8,128)(2,1)}, u32[]{:S(2)}) copy-start(bf16[128,2048]{1,0:T(8,128)(2,1)} %param.19) | copy-start | bytes 1572868
  7.2 53.4 %all-gather.3.cloned.1.call-start = ((), (), s32[]{:S(2)}) async-start(), calls=%async_computation.2 | async-start | bytes 2621440 | tf_op jit(solution)/shard_map/all_gather | solution.py:58
  11.4 109.8 %all-gather.5.cloned.1.call-start = ((), (), s32[]{:S(2)}) async-start(), calls=%async_computation.3 | async-start | bytes 10485760 | tf_op jit(solution)/shard_map/all_gather | solution.py:108
  11.9 13.0 %collective-permute-start.2 = (bf16[128,2048]{1,0:T(8,128)(2,1)S(1)}, bf16[128,2048]{1,0:T(8,128)(2,1)S(1)}, u32[]{:S(2)}, u32[]{:S(2)}) collective-permute-start(bf16[128,2048]{1,0:T(8,128)(2,1)S(1)} %fusion.5), channel_id=1, source_target_pairs={{0,12},{4,0},{8,4},{12,8},{1,13},{5,1},{9,5},{13,9},{2,14},{6,2},{... | collective-permute-start | bytes 1572872 | tf_op jit(solution)/shard_map/ppermute | solution.py:19
  11.9 35.9 %collective-permute-start.1 = (bf16[128,2048]{1,0:T(8,128)(2,1)S(1)}, bf16[128,2048]{1,0:T(8,128)(2,1)S(1)}, u32[]{:S(2)}, u32[]{:S(2)}) collective-permute-start(bf16[128,2048]{1,0:T(8,128)(2,1)S(1)} %fusion.5), channel_id=1, source_target_pairs={{0,8},{4,12},{8,0},{12,4},{1,9},{5,13},{9,1},{13,5},{2,10},{6,14},... | collective-permute-start | bytes 1572872 | tf_op jit(solution)/shard_map/ppermute | solution.py:19
  14.4 44.7 %collective-permute-start = (bf16[128,2048]{1,0:T(8,128)(2,1)S(1)}, bf16[128,2048]{1,0:T(8,128)(2,1)S(1)}, u32[]{:S(2)}, u32[]{:S(2)}) collective-permute-start(bf16[128,2048]{1,0:T(8,128)(2,1)S(1)} %fusion.5), channel_id=1, source_target_pairs={{0,4},{4,8},{8,12},{12,0},{1,5},{5,9},{9,13},{13,1},{2,6},{6,10},{... | collective-permute-start | bytes 1572872 | tf_op jit(solution)/shard_map/ppermute | solution.py:19
  60.6 0.7 copy-start.5
  60.6 0.7 copy-start.7
  60.6 60.5 %copy-start.9 = (bf16[1,2048,256]{2,1,0:T(8,128)(2,1)S(1)}, bf16[1,2048,256]{2,1,0:T(8,128)(2,1)}, u32[]{:S(2)}) copy-start(bf16[1,2048,256]{2,1,0:T(8,128)(2,1)} %param.23) | copy-start | bytes 3145732
  60.7 152.4 %reduce-scatter.3.cloned.1.call-start = ((), (), s32[]{:S(2)}) async-start(), calls=%async_computation.4 | async-start | bytes 10485760 | tf_op jit(solution)/shard_map/reduce_scatter | solution.py:110
  142.1 123.2 %reduce-scatter.5.cloned.1.call-start = ((), (), s32[]{:S(2)}) async-start(), calls=%async_computation.5 | async-start | bytes 2621440 | tf_op jit(solution)/shard_map/reduce_scatter | solution.py:116
  142.1 7.6 %copy-start.6 = (bf16[512]{0:T(512)(128)(2,1)S(1)}, bf16[512]{0:T(512)(128)(2,1)}, u32[]{:S(2)}) copy-start(bf16[512]{0:T(512)(128)(2,1)} %param.17) | copy-start | bytes 3076
  146.6 3.1 %copy-start.8 = (bf16[512,512]{1,0:T(8,128)(2,1)}, bf16[512,512]{1,0:T(8,128)(2,1)S(1)}, u32[]{:S(2)}) copy-start(bf16[512,512]{1,0:T(8,128)(2,1)S(1)} %get-tuple-element.20) | copy-start | bytes 1572868
  146.6 4.5 %collective-permute-start.3 = (bf16[16,512]{1,0:T(8,128)(2,1)S(1)}, bf16[16,512]{1,0:T(8,128)(2,1)S(1)}, u32[]{:S(2)}, u32[]{:S(2)}) collective-permute-start(bf16[16,512]{1,0:T(8,128)(2,1)S(1)} %slice.72), channel_id=1, source_target_pairs={{0,4},{4,8},{8,12},{1,5},{5,9},{9,13},{2,6},{6,10},{10,14},{3,7},{... | collective-permute-start | bytes 49160 | tf_op jit(solution)/shard_map/ppermute | solution.py:12
  153.6 1.0 copy-start.1
  154.7 1.8 copy-start.2
  214.6 12.7 %collective-permute-start.6 = (bf16[128,2048]{1,0:T(8,128)(2,1)S(1)}, bf16[128,2048]{1,0:T(8,128)(2,1)S(1)}, u32[]{:S(2)}, u32[]{:S(2)}) collective-permute-start(bf16[128,2048]{1,0:T(8,128)(2,1)S(1)} %get-tuple-element.11), channel_id=1, source_target_pairs={{0,4},{4,8},{8,12},{12,0},{1,5},{5,9},{9,13},{13,1},{2,6},{6,10},{... | collective-permute-start | bytes 1572872 | tf_op jit(solution)/shard_map/ppermute | solution.py:19
  215.8 44.2 %collective-permute-start.5 = (bf16[128,2048]{1,0:T(8,128)(2,1)S(1)}, bf16[128,2048]{1,0:T(8,128)(2,1)S(1)}, u32[]{:S(2)}, u32[]{:S(2)}) collective-permute-start(bf16[128,2048]{1,0:T(8,128)(2,1)S(1)} %get-tuple-element.12), channel_id=1, source_target_pairs={{0,8},{4,12},{8,0},{12,4},{1,9},{5,13},{9,1},{13,5},{2,10},{6,14},... | collective-permute-start | bytes 1572872 | tf_op jit(solution)/shard_map/ppermute | solution.py:19
  217.0 46.1 %collective-permute-start.4 = (bf16[128,2048]{1,0:T(8,128)(2,1)S(1)}, bf16[128,2048]{1,0:T(8,128)(2,1)S(1)}, u32[]{:S(2)}, u32[]{:S(2)}) collective-permute-start(bf16[128,2048]{1,0:T(8,128)(2,1)S(1)} %get-tuple-element.10), channel_id=1, source_target_pairs={{0,12},{4,0},{8,4},{12,8},{1,13},{5,1},{9,5},{13,9},{2,14},{6,2},{... | collective-permute-start | bytes 1572872 | tf_op jit(solution)/shard_map/ppermute | solution.py:19
Sparse Core Ops, SparseCore 0:
  11.5 24.0 all-gather.2
  60.8 60.3 all-gather.4
  142.2 70.7 reduce-scatter.2
  216.0 31.1 reduce-scatter.4
